TPU v7x, 32 devices: a whole 2x2x4 slice. The times are simulated.
32 devices in a mesh: grp: 2 (over y), sp: 4 (over z), tp: 4 (over x, core).
Axes of the slice: x: 2, y: 2, z: 4, core: 2. Of those that a mesh axis runs over, the one named last changes fastest.
Arguments:
- resid: bfloat16 [4096, 2048], P(('grp', 'sp', 'tp')), parts along dimension 0, may hold values from -6 to 6
- pool_input: bfloat16 [4096, 512], P(('grp', 'sp'), 'tp'), parts along dimension 0, may hold values from -6 to 6
- group_map: bfloat16 [4, 128, 128], P('tp'), may hold values from -0.5 to 0.5
- pool_scale: bfloat16 [512], P('tp'), may hold values from 0.099609375 to 1.8984375
- out_proj: bfloat16 [512, 2048], P('tp'), may hold values from -0.25 to 0.25
- norm_gain: bfloat16 [2048], replicated, may hold values from 0.099609375 to 1.8984375
- routes: int32 [4096, 2], P(('grp', 'sp', 'tp')), parts along dimension 0, may hold values from 0 to 3, all different within a row; in each aligned block of 128 rows (0 to 127, 128 to 255, ...) at most 80 rows name the same one
- route_weight: float32 [4096, 2], P(('grp', 'sp', 'tp')), parts along dimension 0, may hold values from 0.2 to 1
- expert_gate: bfloat16 [4, 2048, 3584], P('sp', None, 'tp'), may hold values from -0.125 to 0.125
- expert_up: bfloat16 [4, 2048, 3584], P('sp', None, 'tp'), may hold values from -0.125 to 0.125
- expert_down: bfloat16 [4, 3584, 2048], P('sp', 'tp'), may hold values from -0.09375 to 0.09375
Outputs:
- layer_out: bfloat16 [4096, 2048], P(('grp', 'sp', 'tp')), parts along dimension 0
There are 2 independent parts, one for each index of `grp`. A program takes and returns all parts, laid end to end along the dimension named above; an argument that names none is the same for every part. Nothing has to cross between parts.
Inputs may be any that keep to these rules, and one draw needn't show every extreme that they name: The 2 routes of a token differ. Among the tokens of one device (aligned blocks of 128 tokens), no expert is named more than 80 times, and in every draw some device names some expert exactly 80 times.
All inputs are finite; a program needn't handle non-finite values.
Results may differ from a plain program's by a relative error of at most 0.011.
Values may be sent and summed in bfloat16 or wider, within the bound.
A program may use at most 128 MiB of HBM per device.

v0:
```python
import functools

import jax
import jax.numpy as jnp
from jax import lax
from jax.experimental import pallas as pl
from jax.experimental.pallas import tpu as pltpu
from jax.sharding import PartitionSpec as P

GROUPS = 4
norm_eps = 1e-06
BF = jnp.bfloat16
F32 = jnp.float32
MESH = pl.DeviceIdType.MESH
RIM = 2**GROUPS


def nearest(s, j, S):
    low = jnp.minimum(s, S - 1 - s)
    half = (j + 1) // 2
    both = half * (2 * lax.rem(j, 2) - 1)
    rest = (j - low) * (1 - 2 * ((2 * s) // S))
    return s + jnp.where(j <= 2 * low, both * (1 - 2 * ((2 * s) // S)), rest)


def kernel(
    S, T, R, SL,
    resid, pool, gmap, scale, oproj, gain, routes_t, weight_t, wg, wu, wd,
    out,
    wgu_v, wd_v, opj, rim, piece, gout, stage, inbox, pbuf, rbuf, fbuf, fin, ret,
    acc, hid, mixed_v, normed_v,
    w_sem, o_far_s, o_far_r, o_near_s, o_near_r, rim_s, rim_r, pc_s, pc_r,
    z_s, z_r, f_s, f_r, n_s, n_r, pn_s, pn_r, pf_s, pf_r, rz_s, rz_r,
):
    s = lax.axis_index("sp")
    t = lax.axis_index("tp")
    H = T // 2
    D = resid.shape[1]
    F = wd.shape[0]
    near = t + 1 - 2 * lax.rem(t, 2)

    def up(k):
        return lax.rem(t + 2 * k, T)

    def down(base, k):
        return lax.rem(base - 2 * k + 2 * T, T)

    def remote(src, dst, ss, rs, sp=None, tp=None):
        return pltpu.make_async_remote_copy(
            src_ref=src, dst_ref=dst, send_sem=ss, recv_sem=rs,
            device_id={"sp": s if sp is None else sp, "tp": t if tp is None else tp},
            device_id_type=MESH,
        )

    loads = [
        pltpu.make_async_copy(wg, wgu_v.at[:, pl.ds(0, F)], w_sem.at[0]),
        pltpu.make_async_copy(wu, wgu_v.at[:, pl.ds(F, F)], w_sem.at[1]),
        pltpu.make_async_copy(wd, wd_v, w_sem.at[2]),
    ]
    for load in loads:
        load.start()

    barrier = pltpu.get_barrier_semaphore()

    @pl.loop(1, S)
    def _(j):
        pl.semaphore_signal(
            barrier, inc=1, device_id={"sp": lax.rem(s + j, S), "tp": t}, device_id_type=MESH
        )

    for j in range(1, T):
        pl.semaphore_signal(
            barrier, inc=1, device_id={"sp": s, "tp": lax.rem(t + j, T)}, device_id_type=MESH
        )
    pl.semaphore_wait(barrier, S - 1 + T - 1)

    seq = pool.shape[0]
    rim_copy = remote(
        pool.at[pl.ds(seq - RIM, RIM)], rim, rim_s.at[0], rim_r.at[0], sp=lax.rem(s + 1, S)
    )
    rim_copy.start()

    def o_far(k):
        return remote(oproj, opj.at[t], o_far_s.at[k], o_far_r.at[k], tp=up(k))

    def o_near(k):
        block = down(t, k)
        return remote(
            oproj if k == 0 else opj.at[block], opj.at[block], o_near_s.at[k], o_near_r.at[k],
            tp=near,
        )

    for k in range(1, H):
        o_far(k).start()
    o_near(0).start()

    E = S
    EP = max(8, E)
    e_row = lax.broadcasted_iota(jnp.int32, (EP, R), 0)
    hot_row = [e_row == routes_t[k : k + 1, :] for k in range(2)]
    both_row = jnp.where(hot_row[0] | hot_row[1], 1.0, 0.0).astype(BF)
    before = lax.broadcasted_iota(jnp.int32, (R, R), 0) < lax.broadcasted_iota(
        jnp.int32, (R, R), 1
    )
    rank_row = jnp.dot(both_row, jnp.where(before, 1.0, 0.0).astype(BF), preferred_element_type=F32)
    slot_row = rank_row + (e_row * SL).astype(F32)
    tgt_row = [jnp.sum(jnp.where(h, slot_row, 0.0), axis=0, keepdims=True) for h in hot_row]

    eye = lax.broadcasted_iota(jnp.int32, (R, R), 0) == lax.broadcasted_iota(
        jnp.int32, (R, R), 1
    )

    def column(row):
        return jnp.sum(jnp.where(eye, row, 0.0), axis=1, keepdims=True)

    tgt_col = [column(row) for row in tgt_row]
    weight_col = [column(weight_t[k : k + 1, :]) for k in range(2)]

    rim_copy.wait_recv()
    values = pool[...].astype(F32)
    rim_v = jnp.where(s > 0, rim[...].astype(F32), 0.0)
    run = jnp.concatenate([rim_v, values], axis=0)
    window_sum = None
    for g in range(GROUPS):
        run = run + pltpu.roll(run, 2**g, 0)
        part = run[RIM:]
        window_sum = part if g == 0 else jnp.where(t >= g, part, window_sum)
    window = jnp.int32(2)
    for g in range(1, GROUPS):
        window = jnp.where(t >= g, jnp.int32(2 ** (g + 1)), window)
    position = s * seq + 1 + lax.broadcasted_iota(jnp.int32, (seq, 128), 0)
    divisor = jnp.minimum(position, window).astype(F32)
    pooled = (window_sum / divisor - values).astype(BF)
    product = jnp.dot(pooled, gmap[0], preferred_element_type=F32)
    piece[...] = (product * scale[...].astype(F32)).astype(BF).reshape(T, R, 128)

    def piece_copy(j):
        q = lax.rem(t + j, T)
        return remote(piece.at[q], gout.at[t], pc_s.at[j], pc_r.at[j], tp=q)

    for j in range(1, T):
        piece_copy(j).start()

    for k in range(1, H):
        o_far(k).wait_recv()
        o_near(k).start()

    for j in range(1, T):
        piece_copy(j).wait_recv()
    for k in range(H):
        o_near(k).wait_recv()

    gout[t] = piece[t]
    opj[t] = oproj[...]
    mix = resid[...].astype(F32)
    total = jnp.dot(gout[0], opj[0], preferred_element_type=F32)
    for q in range(1, T):
        total = total + jnp.dot(gout[q], opj[q], preferred_element_type=F32)
    mixed = (mix + total).astype(BF)
    mixed_v[...] = mixed
    residual = mixed.astype(F32)
    scaled = residual * lax.rsqrt(jnp.mean(residual * residual, axis=1, keepdims=True) + norm_eps)
    normed_v[...] = (scaled * gain[...].astype(F32).reshape(1, D)).astype(BF)

    slot_iota = lax.broadcasted_iota(jnp.int32, (SL, R), 0)

    def rows_of(e):
        want = (slot_iota + e * SL).astype(F32)
        place = jnp.where((tgt_row[0] == want) | (tgt_row[1] == want), 1.0, 0.0).astype(BF)
        return jnp.dot(place, normed_v[...], preferred_element_type=F32).astype(BF)

    def dest(j):
        return nearest(s, S - j, S)

    def source(j):
        return nearest(s, lax.rem(S - j, S), S)

    def z_copy(e):
        return remote(stage.at[e], inbox.at[s, t], z_s.at[e], z_r.at[s], sp=e)

    def z_arrival(i):
        return remote(stage.at[i], inbox.at[i, t], z_s.at[i], z_r.at[i], sp=i)

    def far_copy(j, k):
        block = inbox.at[source(j), t]
        return remote(block, block, f_s.at[j, k], f_r.at[j, k], tp=up(k))

    def near_copy(j, k):
        block = inbox.at[source(j), down(t, k)]
        return remote(block, block, n_s.at[j, k], n_r.at[j, k], tp=near)

    def forward_own(j):
        for k in range(1, H):
            far_copy(j, k).start()
        near_copy(j, 0).start()

    def p_near(j, k):
        return remote(
            pbuf.at[j, down(near, k)], rbuf.at[j, k], pn_s.at[j, k], pn_r.at[j, k], tp=near
        )

    def p_far(j, k):
        q = down(t, k)
        return remote(pbuf.at[j, q], fbuf.at[j, k], pf_s.at[j, k], pf_r.at[j, k], tp=q)

    def back(j):
        return remote(fin.at[j], ret.at[s], rz_s.at[j], rz_r.at[s], sp=source(j))

    def back_arrival(j):
        e = source(j)
        return remote(fin.at[j], ret.at[e], rz_s.at[j], rz_r.at[e], sp=e)

    inbox[s, t] = rows_of(s)
    forward_own(0)

    @pl.loop(1, S)
    def _(j):
        e = dest(j)
        stage[e] = rows_of(e)
        z_copy(e).start()

    for load in loads:
        load.wait()

    def arrive(j):
        z_arrival(source(j)).wait_recv()
        forward_own(j)

    NT = 256 if (2 * F) % 256 == 0 else 128
    DT = 256 if D % 256 == 0 else 128

    @pl.loop(0, S + 2)
    def _(j):
        @pl.when((j + 1 < S) & (j + 1 > 0))
        def _():
            arrive(j + 1)

        @pl.when((j >= 1) & (j <= S))
        def _():
            i = j - 1
            for k in range(H):
                p_near(i, k).wait_recv()
            for k in range(1, H):
                q = down(t, k)
                pbuf[i, q] = (pbuf[i, q].astype(F32) + rbuf[i, k].astype(F32)).astype(BF)
                p_far(i, k).start()

        @pl.when(j < S)
        def _():
            for k in range(1, H):
                far_copy(j, k).wait_recv()
                near_copy(j, k).start()

        @pl.when(j >= 2)
        def _():
            i = j - 2
            value = pbuf[i, t].astype(F32) + rbuf[i, 0].astype(F32)
            for k in range(1, H):
                p_far(i, k).wait_recv()
                value = value + fbuf[i, k].astype(F32)
            fin[i] = value.astype(BF)

            @pl.when(i > 0)
            def _():
                back(i).start()

        @pl.when(j < S)
        def _():
            for k in range(H):
                near_copy(j, k).wait_recv()
            src = source(j)

            @pl.loop(0, 2 * F // NT)
            def _(n):
                cols = pl.ds(pl.multiple_of(n * NT, NT), NT)
                x = inbox[src].reshape(T * SL, D)
                acc[:, cols] = jnp.dot(x, wgu_v[:, cols], preferred_element_type=F32)

            gate = acc[:, :F]
            hid[...] = (gate / (1.0 + jnp.exp(-gate)) * acc[:, F:]).astype(BF)

            @pl.loop(0, D // DT)
            def _(n):
                cols = pl.ds(pl.multiple_of(n * DT, DT), DT)
                y = jnp.dot(hid[...], wd_v[:, cols], preferred_element_type=F32)
                pbuf[j, :, :, cols] = y.astype(BF).reshape(T, SL, DT)

            for k in range(H):
                p_near(j, k).start()

    @pl.loop(1, S)
    def _(j):
        back_arrival(j).wait_recv()

    ret[s] = fin[0]
    flat = ret[...].reshape(S * SL, D)
    lanes = lax.broadcasted_iota(jnp.int32, (R, S * SL), 1).astype(F32)
    total = mixed_v[...].astype(F32)
    picked = [
        weight_col[k]
        * jnp.dot(
            jnp.where(tgt_col[k] == lanes, 1.0, 0.0).astype(BF), flat, preferred_element_type=F32
        )
        for k in range(2)
    ]
    out[...] = (total + (picked[0] + picked[1])).astype(BF)

    rim_copy.wait_send()
    for k in range(1, H):
        o_far(k).wait_send()
    for k in range(H):
        o_near(k).wait_send()
    for j in range(1, T):
        piece_copy(j).wait_send()

    @pl.loop(0, S)
    def _(j):
        for k in range(1, H):
            far_copy(j, k).wait_send()
            p_far(j, k).wait_send()
        for k in range(H):
            near_copy(j, k).wait_send()
            p_near(j, k).wait_send()

    @pl.loop(1, S)
    def _(j):
        z_copy(dest(j)).wait_send()
        back(j).wait_send()


def local(
    resid, pool_input, group_map, pool_scale, out_proj, norm_gain, routes, route_weight,
    expert_gate, expert_up, expert_down,
):
    S, T = lax.axis_size("sp"), lax.axis_size("tp")
    R, D = resid.shape
    H = T // 2
    top = routes.shape[1]
    experts = S * expert_gate.shape[0]
    slots = max(2, 5 * R * top // (4 * experts))
    SL = -(-slots // 16) * 16
    F = expert_down.shape[1]
    GD = group_map.shape[1]
    vmem, hbm = pl.BlockSpec(memory_space=pltpu.VMEM), pl.BlockSpec(memory_space=pl.ANY)
    dma = lambda *n: pltpu.SemaphoreType.DMA(n)
    buf = lambda *n: pltpu.VMEM(n, BF)
    return pl.pallas_call(
        functools.partial(kernel, S, T, R, SL),
        out_shape=jax.ShapeDtypeStruct((R, D), BF),
        in_specs=[vmem] * 8 + [hbm] * 3,
        out_specs=vmem,
        scratch_shapes=[
            buf(D, 2 * F), buf(F, D), buf(T, GD, D), buf(RIM, GD), buf(T, R, GD), buf(T, R, GD),
            buf(S, SL, D), buf(S, T, SL, D), buf(S, T, SL, D), buf(S, H, SL, D), buf(S, H, SL, D),
            buf(S, SL, D), buf(S, SL, D),
            pltpu.VMEM((T * SL, 2 * F), F32), buf(T * SL, F), buf(R, D), buf(R, D),
            dma(3), dma(H), dma(H), dma(H), dma(H), dma(1), dma(1), dma(T), dma(T),
            dma(S), dma(S), dma(S, H), dma(S, H), dma(S, H), dma(S, H),
            dma(S, H), dma(S, H), dma(S, H), dma(S, H), dma(S), dma(S),
        ],
        compiler_params=pltpu.CompilerParams(
            collective_id=0, has_side_effects=True, vmem_limit_bytes=63 * 1024 * 1024
        ),
    )(
        resid, pool_input, group_map, pool_scale.reshape(1, -1), out_proj,
        norm_gain, routes.T, route_weight.T,
        expert_gate[0], expert_up[0], expert_down[0],
    )


def solution(mesh):
    return jax.shard_map(
        local,
        mesh=mesh,
        in_specs=(
            P(("grp", "sp", "tp"), None),
            P(("grp", "sp"), "tp"),
            P("tp", None, None),
            P("tp"),
            P("tp", None),
            P(),
            P(("grp", "sp", "tp"), None),
            P(("grp", "sp", "tp"), None),
            P("sp", None, "tp"),
            P("sp", None, "tp"),
            P("sp", "tp", None),
        ),
        out_specs=P(("grp", "sp", "tp"), None),
        check_vma=False,
    )
```

profile of v0, /device:TPU:13, one launch (start us, length us, event | category | flops | bytes accessed | tf_op | source)
XLA Modules:
  0.0 107.9 jit_solution(13733379328624502053)
XLA Ops:
  0.0 106.0 %shard_map.109 = bf16[128,2048]{1,0:T(8,128)(2,1)} custom-call(bf16[128,2048]{1,0:T(8,128)(2,1)} %resid.1, bf16[512,128]{1,0:T(8,128)(2,1)} %pool.1, bf16[1,128,128]{2,1,0:T(8,128)(2,1)} %gmap.1, bf16[1,128]{1,0:T(2,128)(2,1)} %bitcast.11, bf16[128,2048]{1,0:T(8,128)(2,1)} %oproj.1, bf16[2048]{0:T(1024)(128)(2,1)} %gain.1, s32[2,128]{1,0:T(2,128)} %bitcast.9, ...), custom_call_target="tpu_custom_call" | custom-call | tf_op jit(solution)/shard_map/pallas_call | solution.py:347
  106.1 1.9 %copy.13 = bf16[128,2048]{1,0:T(8,128)(2,1)} copy(bf16[128,2048]{1,0:T(8,128)(2,1)} %shard_map.109) | data formatting | bytes 1048576
where the time goes:
time: 108 us
  Pallas kernels  106 us (98%)
  local copies, waits for them, and re-layouts  1.88 us (2%)
    pallas_call x1, Pallas kernels, local(): pl.pallas_call(functools.partial(kernel, S, T, R, SL), out_shape=jax.Shap...  106 us

commit v1 on v0

v1 whole, which is shorter than its diff:
```python
import functools

import jax
import jax.numpy as jnp
from jax import lax
from jax.experimental import pallas as pl
from jax.experimental.pallas import tpu as pltpu
from jax.sharding import PartitionSpec as P

GROUPS = 4
norm_eps = 1e-06
BF = jnp.bfloat16
F32 = jnp.float32
MESH = pl.DeviceIdType.MESH
RIM = 2**GROUPS
ORDER = ((0, 1, 2, 3), (1, 3, 0, 2), (2, 0, 3, 1), (3, 2, 1, 0))
SENDS = ((0, 2, 1, 3), (1, 3, 0, 2), (2, 0, 3, 1), (3, 1, 2, 0))


def nearest(s, j, S):
    low = jnp.minimum(s, S - 1 - s)
    half = (j + 1) // 2
    both = half * (2 * lax.rem(j, 2) - 1)
    rest = (j - low) * (1 - 2 * ((2 * s) // S))
    return s + jnp.where(j <= 2 * low, both * (1 - 2 * ((2 * s) // S)), rest)


def look_up(table, s, j):
    value = 0
    for a, row in enumerate(table):
        for b, entry in enumerate(row):
            value = value + jnp.where((s == a) & (j == b), entry, 0)
    return value


def visit(s, j, S):
    return look_up(ORDER, s, j) if S == 4 else nearest(s, lax.rem(S - j, S), S)


def sends(s, j, S):
    return look_up(SENDS, s, j) if S == 4 else nearest(s, S - j, S)


def kernel(
    G, S, T, R, SL, NC,
    resid, pool, gmap, scale, oproj, gain, routes_t, weight_t, wg, wu, wd,
    out,
    wgu_v, wd_v, opj, rim, piece, gout, stage, inbox, pbuf, rbuf, fbuf, fin, ret,
    acc, hid, mixed_v, cast_v, rsend, rin,
    w_sem, ox_s, ox_r, oy_s, oy_r, on_s, on_r, rim_s, rim_r, pc_s, pc_r,
    z_s, z_r, f_s, f_r, n_s, n_r, pn_s, pn_r, pf_s, pf_r, rz_s, rz_r, rr_s, rr_r,
):
    g = lax.axis_index("grp")
    s = lax.axis_index("sp")
    t = lax.axis_index("tp")
    H = T // 2
    D = resid.shape[1]
    F = wd.shape[0]
    DC = D // NC
    GD = oproj.shape[0]
    GH = GD // G
    C = range(NC)
    near = t + 1 - 2 * lax.rem(t, 2)
    inner = (s != 0) & (s != S - 1)

    def cut(c):
        return slice(c * DC, (c + 1) * DC)

    def up(k):
        return lax.rem(t + 2 * k, T)

    def down(base, k):
        return lax.rem(base - 2 * k + 2 * T, T)

    def remote(src, dst, ss, rs, sp=None, tp=None, grp=None):
        return pltpu.make_async_remote_copy(
            src_ref=src, dst_ref=dst, send_sem=ss, recv_sem=rs,
            device_id={
                "grp": g if grp is None else grp,
                "sp": s if sp is None else sp,
                "tp": t if tp is None else tp,
            },
            device_id_type=MESH,
        )

    loads = [
        pltpu.make_async_copy(wg, wgu_v.at[:, pl.ds(0, F)], w_sem.at[0]),
        pltpu.make_async_copy(wu, wgu_v.at[:, pl.ds(F, F)], w_sem.at[1]),
        pltpu.make_async_copy(wd, wd_v, w_sem.at[2]),
    ]
    for load in loads:
        load.start()

    barrier = pltpu.get_barrier_semaphore()

    @pl.loop(1, S * T)
    def _(j):
        peer = lax.rem(s * T + t + j, S * T)
        pl.semaphore_signal(
            barrier, inc=1, device_id={"grp": g, "sp": peer // T, "tp": lax.rem(peer, T)},
            device_id_type=MESH,
        )

    for j in range(1, G):
        pl.semaphore_signal(
            barrier, inc=1, device_id={"grp": lax.rem(g + j, G), "sp": s, "tp": t},
            device_id_type=MESH,
        )
    pl.semaphore_wait(barrier, S * T - 1 + G - 1)

    seq = pool.shape[0]
    rim_copy = remote(
        pool.at[pl.ds(seq - RIM, RIM)], rim, rim_s.at[0], rim_r.at[0], sp=lax.rem(s + 1, S)
    )
    rim_copy.start()

    def own_rows(h):
        return pl.ds(pl.multiple_of(h * GH, GH), GH)

    def o_far(k, c):
        return remote(
            oproj.at[own_rows(g), cut(c)], opj.at[c, t, own_rows(g)],
            ox_s.at[k, c], ox_r.at[k, c], tp=up(k),
        )

    def o_part(k, j, c):
        part = opj.at[c, down(t, k), own_rows(g)]
        return remote(part, part, oy_s.at[k, j, c], oy_r.at[k, j, c], grp=lax.rem(g + j, G))

    def o_near(k, c):
        block = opj.at[c, down(t, k)]
        return remote(
            oproj.at[:, cut(c)] if k == 0 else block, block, on_s.at[k, c], on_r.at[k, c], tp=near
        )

    def o_spread(c):
        for k in range(1, H):
            o_far(k, c).wait_recv()
            for j in range(1, G):
                o_part(k, j, c).start()

    def o_pass(c):
        for k in range(1, H):
            for j in range(1, G):
                o_part(k, j, c).wait_recv()
            o_near(k, c).start()

    for c in range(NC - 1):
        for k in range(1, H):
            o_far(k, c).start()
    for c in C:
        o_near(0, c).start()

    E = S
    EP = max(8, E)
    e_row = lax.broadcasted_iota(jnp.int32, (EP, R), 0)
    hot_row = [e_row == routes_t[k : k + 1, :] for k in range(2)]
    both_row = jnp.where(hot_row[0] | hot_row[1], 1.0, 0.0).astype(BF)
    before = lax.broadcasted_iota(jnp.int32, (R, R), 0) < lax.broadcasted_iota(
        jnp.int32, (R, R), 1
    )
    rank_row = jnp.dot(both_row, jnp.where(before, 1.0, 0.0).astype(BF), preferred_element_type=F32)
    slot_row = rank_row + (e_row * SL).astype(F32)
    tgt_row = [jnp.sum(jnp.where(h, slot_row, 0.0), axis=0, keepdims=True) for h in hot_row]

    eye = lax.broadcasted_iota(jnp.int32, (R, R), 0) == lax.broadcasted_iota(
        jnp.int32, (R, R), 1
    )

    def column(row):
        return jnp.sum(jnp.where(eye, row, 0.0), axis=1, keepdims=True)

    tgt_col = [column(row) for row in tgt_row]
    weight_col = [column(weight_t[k : k + 1, :]) for k in range(2)]

    rim_copy.wait_recv()
    values = pool[...].astype(F32)
    rim_v = jnp.where(s > 0, rim[...].astype(F32), 0.0)
    run = jnp.concatenate([rim_v, values], axis=0)
    window_sum = None
    for n in range(GROUPS):
        run = run + pltpu.roll(run, 2**n, 0)
        part = run[RIM:]
        window_sum = part if n == 0 else jnp.where(t >= n, part, window_sum)
    window = jnp.int32(2)
    for n in range(1, GROUPS):
        window = jnp.where(t >= n, jnp.int32(2 ** (n + 1)), window)
    position = s * seq + 1 + lax.broadcasted_iota(jnp.int32, (seq, GD), 0)
    divisor = jnp.minimum(position, window).astype(F32)
    pooled = (window_sum / divisor - values).astype(BF)
    product = jnp.dot(pooled, gmap[0], preferred_element_type=F32)
    piece[...] = (product * scale[...].astype(F32)).astype(BF).reshape(T, R, GD)

    def piece_copy(j):
        q = lax.rem(t + j, T)
        return remote(piece.at[q], gout.at[t], pc_s.at[j], pc_r.at[j], tp=q)

    for j in range(1, T):
        piece_copy(j).start()
    for k in range(1, H):
        o_far(k, NC - 1).start()
    gout[t] = piece[t]
    for c in C:
        opj[c, t] = oproj[:, cut(c)]

    slots = S * SL
    slot_iota = lax.broadcasted_iota(jnp.int32, (slots, R), 0).astype(F32)
    place = jnp.where((tgt_row[0] == slot_iota) | (tgt_row[1] == slot_iota), 1.0, 0.0).astype(BF)

    def z_copy(e, c):
        return remote(stage.at[c, e], inbox.at[s, c, t], z_s.at[e, c], z_r.at[s, c], sp=e)

    def z_arrival(i, c):
        return remote(stage.at[c, i], inbox.at[i, c, t], z_s.at[i, c], z_r.at[i, c], sp=i)

    def far_copy(i, k, c):
        block = inbox.at[i, c, t]
        return remote(block, block, f_s.at[i, k, c], f_r.at[i, k, c], tp=up(k))

    def near_copy(i, k, c):
        block = inbox.at[i, c, down(t, k)]
        return remote(block, block, n_s.at[i, k, c], n_r.at[i, k, c], tp=near)

    def r_copy(e, q):
        return remote(rsend.at[e], rin.at[s, t], rr_s.at[e, q], rr_r.at[s, t], sp=e, tp=q)

    def r_arrival(i, q):
        return remote(rsend.at[i], rin.at[i, q], rr_s.at[i, q], rr_r.at[i, q], sp=i, tp=q)

    def p_near(i, k, c):
        return remote(
            pbuf.at[i, c, down(near, k)], rbuf.at[i, k, c], pn_s.at[i, k, c], pn_r.at[i, k, c],
            tp=near,
        )

    def p_far(i, k, c):
        q = down(t, k)
        return remote(pbuf.at[i, c, q], fbuf.at[i, k, c], pf_s.at[i, k, c], pf_r.at[i, k, c], tp=q)

    def back(i, c):
        return remote(fin.at[i, c], ret.at[c, s], rz_s.at[i, c], rz_r.at[s, c], sp=i)

    def back_arrival(e, c):
        return remote(fin.at[e, c], ret.at[c, e], rz_s.at[e, c], rz_r.at[e, c], sp=e)

    def push(i, c):
        for k in range(1, H):
            far_copy(i, k, c).start()
        near_copy(i, 0, c).start()

    def fwd(p, c):
        i = visit(s, p, S)
        z_arrival(i, c).wait_recv()
        push(i, c)

    def relay(p, c):
        i = visit(s, p, S)
        for k in range(1, H):
            far_copy(i, k, c).wait_recv()
            near_copy(i, k, c).start()

    def ready(p):
        i = visit(s, p, S)
        for c in C:
            for k in range(H):
                near_copy(i, k, c).wait_recv()

        @pl.loop(0, T)
        def _(q):
            @pl.when((i != s) | (q != t))
            def _():
                r_arrival(i, q).wait_recv()

    NT = 256 if (2 * F) % 256 == 0 else 128
    DT = 512
    GN = 2 * F // NT

    def hidden(p, lo, hi):
        i = visit(s, p, S)

        def one(n):
            cols = pl.ds(pl.multiple_of(n * NT, NT), NT)
            total = None
            for c in C:
                x = inbox[i, c].reshape(T * SL, DC)
                y = jnp.dot(x, wgu_v[cut(c), cols], preferred_element_type=F32)
                total = y if total is None else total + y
            acc[:, cols] = total

        for n in range(lo, hi):
            one(n)

    def gated(p):
        i = visit(s, p, S)
        spot = lax.broadcasted_iota(jnp.int32, (SL, 128), 0) == lax.broadcasted_iota(
            jnp.int32, (SL, 128), 1
        )
        for q in range(T):
            rows = slice(q * SL, (q + 1) * SL)
            r = jnp.sum(jnp.where(spot, rin[i, q], 0.0), axis=1, keepdims=True)
            gate = acc[rows, :F] * r
            hid[rows] = (gate / (1.0 + jnp.exp(-gate)) * (acc[rows, F:] * r)).astype(BF)

    def lower(p, c):
        i = visit(s, p, S)

        for n in range(DC // DT):
            y = jnp.dot(
                hid[...], wd_v[:, c * DC + n * DT : c * DC + (n + 1) * DT],
                preferred_element_type=F32,
            )
            pbuf[i, c, :, :, n * DT : (n + 1) * DT] = y.astype(BF).reshape(T, SL, DT)

        for k in range(H):
            p_near(i, k, c).start()

    def pair(p, c):
        i = visit(s, p, S)
        for k in range(H):
            p_near(i, k, c).wait_recv()
        for k in range(1, H):
            q = down(t, k)
            pbuf[i, c, q] = (pbuf[i, c, q].astype(F32) + rbuf[i, k, c].astype(F32)).astype(BF)
            p_far(i, k, c).start()

    def finish(p, c):
        i = visit(s, p, S)
        value = pbuf[i, c, t].astype(F32) + rbuf[i, 0, c].astype(F32)
        for k in range(1, H):
            p_far(i, k, c).wait_recv()
            value = value + fbuf[i, k, c].astype(F32)
        return i, value.astype(BF)

    def send_back(p, c):
        i, value = finish(p, c)
        fin[i, c] = value
        back(i, c).start()

    def only(where, act, p, *c):
        @pl.when(where)
        def _():
            for n in c:
                act(p, n)

    def mix_part(c, wide, square):
        for k in range(H):
            o_near(k, c).wait_recv()
        total = jnp.dot(wide, opj[c].reshape(T * GD, DC), preferred_element_type=F32)
        mixed = (resid[:, cut(c)].astype(F32) + total).astype(BF)
        mixed_v[:, cut(c)] = mixed
        residual = mixed.astype(F32)
        cast = (residual * gain[cut(c)].astype(F32).reshape(1, DC)).astype(BF)
        stage[c] = jnp.dot(place, cast, preferred_element_type=F32).astype(BF).reshape(S, SL, DC)
        inbox[s, c, t] = stage[c, s]

        z_copy(sends(s, 1, S), c).start()

        @pl.when(inner)
        def _():
            z_copy(sends(s, 2, S), c).start()

        push(s, c)
        return square + jnp.sum(residual * residual, axis=1, keepdims=True)

    square = jnp.zeros((R, 1), F32)
    o_spread(0)
    o_spread(1)
    for c in range(2, NC):
        o_pass(c - 2)
        o_spread(c)
    for j in range(1, T):
        piece_copy(j).wait_recv()
    wide = jnp.concatenate([gout[q] for q in range(T)], axis=1)
    for c in C:
        square = mix_part(c, wide, square)
        if c + 2 < NC:
            o_pass(c + NC - 2)
    unit = lax.rsqrt(square * (1.0 / D) + norm_eps)

    @pl.loop(0, S)
    def _(e):
        lane = (lax.broadcasted_iota(jnp.int32, (R, 128), 1) + e * SL).astype(F32)
        inside = lax.broadcasted_iota(jnp.int32, (R, 128), 1) < SL
        mine = ((tgt_col[0] == lane) | (tgt_col[1] == lane)) & inside
        rsend[e] = jnp.sum(jnp.where(mine, unit, 0.0), axis=0, keepdims=True)

    rin[s, t] = rsend[s]

    @pl.loop(1, S * T)
    def _(j):
        peer = lax.rem(s * T + t + j, S * T)
        r_copy(peer // T, lax.rem(peer, T)).start()

    @pl.loop(jnp.where(inner, 3, 2), S)
    def _(j):
        for c in C:
            z_copy(sends(s, j, S), c).start()

    for load in loads:
        load.wait()

    if S == 4:
        edge = (s == 0) | (s == S - 1)
        relay(0, 0)
        fwd(1, 0)
        relay(0, 1)
        fwd(1, 1)
        relay(0, 2)
        fwd(1, 2)
        relay(0, 3)
        ready(0)
        hidden(0, 0, 3)
        fwd(1, 3)
        relay(1, 0)
        hidden(0, 3, 5)
        relay(1, 1)
        hidden(0, 5, 7)
        fwd(2, 0)
        gated(0)
        lower(0, 0)
        relay(1, 2)
        lower(0, 1)
        fwd(2, 1)
        lower(0, 2)
        lower(0, 3)
        fwd(2, 2)
        relay(1, 3)
        ready(1)
        hidden(1, 0, 3)
        fwd(2, 3)
        relay(2, 0)
        hidden(1, 3, 5)
        relay(2, 1)
        hidden(1, 5, 7)
        only(edge, fwd, 3, 0)
        relay(2, 2)
        gated(1)
        lower(1, 0)
        only(edge, fwd, 3, 1)
        lower(1, 1)
        lower(1, 2)
        only(inner, pair, 1, 0)
        relay(2, 3)
        lower(1, 3)
        only(inner, pair, 1, 1)
        only(edge, fwd, 3, 2)
        only(inner, pair, 1, 2, 3)
        only(edge, fwd, 3, 3)
        ready(2)
        hidden(2, 0, 3)
        only(inner, send_back, 1, 0)
        only(edge, relay, 3, 0)
        only(inner, fwd, 3, 0)
        hidden(2, 3, 5)
        only(edge, relay, 3, 1)
        only(inner, fwd, 3, 1)
        only(inner, send_back, 1, 1)
        hidden(2, 5, 7)
        gated(2)
        only(edge, relay, 3, 2)
        only(inner, fwd, 3, 2)
        only(inner, send_back, 1, 2)
        lower(2, 0)
        lower(2, 1)
        only(edge, pair, 2, 0)
        lower(2, 2)
        only(edge, pair, 2, 1)
        only(edge, relay, 3, 3)
        only(inner, fwd, 3, 3)
        lower(2, 3)
        only(inner, send_back, 1, 3)
        only(edge, pair, 2, 2, 3)
        only(inner, pair, 2, 0, 1, 2, 3)
        only(inner, relay, 3, 0, 1, 2, 3)
        ready(3)
        hidden(3, 0, 3)
        only(edge, send_back, 2, 0)
        hidden(3, 3, 5)
        only(edge, send_back, 2, 1)
        only(inner, send_back, 2, 0)
        hidden(3, 5, 7)
        gated(3)
        only(edge, send_back, 2, 2)
        only(inner, send_back, 2, 1)
        lower(3, 0)
        lower(3, 1)
        pair(3, 0)
        lower(3, 2)
        pair(3, 1)
        only(inner, send_back, 2, 2)
        lower(3, 3)
        only(edge, send_back, 2, 3)
        pair(3, 2)
        pair(3, 3)
        only(edge, pair, 1, 0, 1, 2, 3)
        pair(0, 0)
        pair(0, 1)
        pair(0, 2)
        pair(0, 3)
        only(inner, send_back, 2, 3)
        send_back(3, 0)
        send_back(3, 1)
        send_back(3, 2)
        send_back(3, 3)
        only(edge, send_back, 1, 0, 1, 2, 3)
    else:
        @pl.loop(0, S + 1)
        def _(j):
            @pl.when(j < S)
            def _():
                for c in C:
                    relay(j, c)

            @pl.when(j + 1 < S)
            def _():
                for c in C:
                    fwd(j + 1, c)

            @pl.when(j > 1)
            def _():
                for c in C:
                    pair(j - 1, c)

            @pl.when(j < S)
            def _():
                ready(j)
                hidden(j, 0, GN)
                gated(j)
                for c in C:
                    lower(j, c)

            @pl.when(j > 1)
            def _():
                for c in C:
                    send_back(j - 1, c)

        for c in C:
            pair(0, c)

    lanes = lax.broadcasted_iota(jnp.int32, (R, slots), 1).astype(F32)
    pick = [jnp.where(tgt_col[k] == lanes, 1.0, 0.0).astype(BF) for k in range(2)]

    for c in C:
        _, value = finish(0, c)
        ret[c, s] = value

        @pl.loop(1, S)
        def _(j):
            back_arrival(visit(s, j, S), c).wait_recv()

        flat = ret[c].reshape(slots, DC)
        total = mixed_v[:, cut(c)].astype(F32)
        picked = [
            weight_col[k] * jnp.dot(pick[k], flat, preferred_element_type=F32) for k in range(2)
        ]
        out[:, cut(c)] = (total + (picked[0] + picked[1])).astype(BF)

    rim_copy.wait_send()
    for c in C:
        for k in range(1, H):
            o_far(k, c).wait_send()
            for j in range(1, G):
                o_part(k, j, c).wait_send()
        for k in range(H):
            o_near(k, c).wait_send()
    for j in range(1, T):
        piece_copy(j).wait_send()

    @pl.loop(0, S)
    def _(i):
        for c in C:
            for k in range(1, H):
                far_copy(i, k, c).wait_send()
                p_far(i, k, c).wait_send()
            for k in range(H):
                near_copy(i, k, c).wait_send()
                p_near(i, k, c).wait_send()

    @pl.loop(1, S)
    def _(j):
        i = visit(s, j, S)
        for c in C:
            z_copy(i, c).wait_send()
            back(i, c).wait_send()

    @pl.loop(1, S * T)
    def _(j):
        peer = lax.rem(s * T + t + j, S * T)
        r_copy(peer // T, lax.rem(peer, T)).wait_send()


def local(
    resid, pool_input, group_map, pool_scale, out_proj, norm_gain, routes, route_weight,
    expert_gate, expert_up, expert_down,
):
    G, S, T = lax.axis_size("grp"), lax.axis_size("sp"), lax.axis_size("tp")
    R, D = resid.shape
    H = T // 2
    top = routes.shape[1]
    experts = S * expert_gate.shape[0]
    room = max(2, 5 * R * top // (4 * experts))
    SL = -(-room // 16) * 16
    F = expert_down.shape[1]
    GD = group_map.shape[1]
    NC = 4
    DC = D // NC
    vmem, hbm = pl.BlockSpec(memory_space=pltpu.VMEM), pl.BlockSpec(memory_space=pl.ANY)
    dma = lambda *n: pltpu.SemaphoreType.DMA(n)
    buf = lambda *n: pltpu.VMEM(n, BF)
    return pl.pallas_call(
        functools.partial(kernel, G, S, T, R, SL, NC),
        out_shape=jax.ShapeDtypeStruct((R, D), BF),
        in_specs=[vmem] * 8 + [hbm] * 3,
        out_specs=vmem,
        scratch_shapes=[
            buf(D, 2 * F), buf(F, D), buf(NC, T, GD, DC), buf(RIM, GD), buf(T, R, GD),
            buf(T, R, GD),
            buf(NC, S, SL, DC), buf(S, NC, T, SL, DC), buf(S, NC, T, SL, DC),
            buf(S, H, NC, SL, DC), buf(S, H, NC, SL, DC), buf(S, NC, SL, DC), buf(NC, S, SL, DC),
            pltpu.VMEM((T * SL, 2 * F), F32), buf(T * SL, F), buf(R, D), buf(R, D),
            pltpu.VMEM((S, 1, 128), F32), pltpu.VMEM((S, T, 1, 128), F32),
            dma(3), dma(H, NC), dma(H, NC), dma(H, G, NC), dma(H, G, NC), dma(H, NC), dma(H, NC),
            dma(1), dma(1), dma(T), dma(T),
            dma(S, NC), dma(S, NC), dma(S, H, NC), dma(S, H, NC), dma(S, H, NC), dma(S, H, NC),
            dma(S, H, NC), dma(S, H, NC), dma(S, H, NC), dma(S, H, NC), dma(S, NC), dma(S, NC),
            dma(S, T), dma(S, T),
        ],
        compiler_params=pltpu.CompilerParams(
            collective_id=0, has_side_effects=True, vmem_limit_bytes=63 * 1024 * 1024
        ),
    )(
        resid, pool_input, group_map, pool_scale.reshape(1, -1), out_proj,
        norm_gain, routes.T, route_weight.T,
        expert_gate[0], expert_up[0], expert_down[0],
    )


def solution(mesh):
    return jax.shard_map(
        local,
        mesh=mesh,
        in_specs=(
            P(("grp", "sp", "tp"), None),
            P(("grp", "sp"), "tp"),
            P("tp", None, None),
            P("tp"),
            P("tp", None),
            P(),
            P(("grp", "sp", "tp"), None),
            P(("grp", "sp", "tp"), None),
            P("sp", None, "tp"),
            P("sp", None, "tp"),
            P("sp", "tp", None),
        ),
        out_specs=P(("grp", "sp", "tp"), None),
        check_vma=False,
    )
```

time: 108 us -> 88.1 us (0.82)
  the two profiles are of different devices: /device:TPU:13 before, /device:TPU:0 now
where the time goes in v1:
time: 88.1 us; the launch traced here: 87.9 us
  Pallas kernels  86 us (98%)
  local copies, waits for them, and re-layouts  1.88 us (2%)
    pallas_call x1, Pallas kernels, local(): pl.pallas_call(functools.partial(kernel, G, S, T, R, SL, NC), out_shape=j...  86 us
    unnamed x1, local copies, waits for them, and re-layouts  1.88 us

profile of v1, /device:TPU:0, one launch (start us, length us, event | category | flops | bytes accessed | tf_op | source)
XLA Modules:
  0.0 87.9 jit_solution(2074891233914842295)
XLA Ops:
  0.0 86.0 %shard_map.109 = bf16[128,2048]{1,0:T(8,128)(2,1)} custom-call(bf16[128,2048]{1,0:T(8,128)(2,1)} %resid.1, bf16[512,128]{1,0:T(8,128)(2,1)} %pool.1, bf16[1,128,128]{2,1,0:T(8,128)(2,1)} %gmap.1, bf16[1,128]{1,0:T(2,128)(2,1)} %bitcast.11, bf16[128,2048]{1,0:T(8,128)(2,1)} %oproj.1, bf16[2048]{0:T(1024)(128)(2,1)} %gain.1, s32[2,128]{1,0:T(2,128)} %bitcast.9, ...), custom_call_target="tpu_custom_call" | custom-call | tf_op jit(solution)/shard_map/pallas_call | solution.py:610
  86.0 1.9 %copy.13 = bf16[128,2048]{1,0:T(8,128)(2,1)} copy(bf16[128,2048]{1,0:T(8,128)(2,1)} %shard_map.109) | data formatting | bytes 1048576

commit v2 on v1

--- a/solution.py
+++ b/solution.py
@@ -46,7 +46,7 @@
     resid, pool, gmap, scale, oproj, gain, routes_t, weight_t, wg, wu, wd,
     out,
     wgu_v, wd_v, opj, rim, piece, gout, stage, inbox, pbuf, rbuf, fbuf, fin, ret,
-    acc, hid, mixed_v, cast_v, rsend, rin,
+    acc, hid, mixed_v, rsend, rin,
     w_sem, ox_s, ox_r, oy_s, oy_r, on_s, on_r, rim_s, rim_r, pc_s, pc_r,
     z_s, z_r, f_s, f_r, n_s, n_r, pn_s, pn_r, pf_s, pf_r, rz_s, rz_r, rr_s, rr_r,
 ):
@@ -120,17 +120,19 @@
     def o_far(k, c):
         return remote(
             oproj.at[own_rows(g), cut(c)], opj.at[c, t, own_rows(g)],
-            ox_s.at[k, c], ox_r.at[k, c], tp=up(k),
+            ox_s.at[k - 1], ox_r.at[k - 1, c], tp=up(k),
         )
 
     def o_part(k, j, c):
         part = opj.at[c, down(t, k), own_rows(g)]
-        return remote(part, part, oy_s.at[k, j, c], oy_r.at[k, j, c], grp=lax.rem(g + j, G))
+        return remote(
+            part, part, oy_s.at[k - 1, j - 1], oy_r.at[k - 1, j - 1, c], grp=lax.rem(g + j, G)
+        )
 
     def o_near(k, c):
         block = opj.at[c, down(t, k)]
         return remote(
-            oproj.at[:, cut(c)] if k == 0 else block, block, on_s.at[k, c], on_r.at[k, c], tp=near
+            oproj.at[:, cut(c)] if k == 0 else block, block, on_s.at[0], on_r.at[c], tp=near
         )
 
     def o_spread(c):
@@ -193,7 +195,7 @@
 
     def piece_copy(j):
         q = lax.rem(t + j, T)
-        return remote(piece.at[q], gout.at[t], pc_s.at[j], pc_r.at[j], tp=q)
+        return remote(piece.at[q], gout.at[t], pc_s.at[0], pc_r.at[0], tp=q)
 
     for j in range(1, T):
         piece_copy(j).start()
@@ -208,40 +210,38 @@
     place = jnp.where((tgt_row[0] == slot_iota) | (tgt_row[1] == slot_iota), 1.0, 0.0).astype(BF)
 
     def z_copy(e, c):
-        return remote(stage.at[c, e], inbox.at[s, c, t], z_s.at[e, c], z_r.at[s, c], sp=e)
+        return remote(stage.at[c, e], inbox.at[s, c, t], z_s.at[0], z_r.at[s, c], sp=e)
 
     def z_arrival(i, c):
-        return remote(stage.at[c, i], inbox.at[i, c, t], z_s.at[i, c], z_r.at[i, c], sp=i)
+        return remote(stage.at[c, i], inbox.at[i, c, t], z_s.at[0], z_r.at[i, c], sp=i)
 
     def far_copy(i, k, c):
         block = inbox.at[i, c, t]
-        return remote(block, block, f_s.at[i, k, c], f_r.at[i, k, c], tp=up(k))
+        return remote(block, block, f_s.at[k - 1], f_r.at[i, k - 1, c], tp=up(k))
 
     def near_copy(i, k, c):
         block = inbox.at[i, c, down(t, k)]
-        return remote(block, block, n_s.at[i, k, c], n_r.at[i, k, c], tp=near)
-
-    def r_copy(e, q):
-        return remote(rsend.at[e], rin.at[s, t], rr_s.at[e, q], rr_r.at[s, t], sp=e, tp=q)
-
-    def r_arrival(i, q):
-        return remote(rsend.at[i], rin.at[i, q], rr_s.at[i, q], rr_r.at[i, q], sp=i, tp=q)
+        return remote(block, block, n_s.at[0], n_r.at[i], tp=near)
+
+    def r_copy(e, q, n):
+        return remote(rsend.at[e], rin.at[s, t], rr_s.at[n], rr_r.at[s], sp=e, tp=q)
+
+    def whole(ref, ss, rs):
+        return remote(ref, ref, ss, rs, tp=near)
 
     def p_near(i, k, c):
         return remote(
-            pbuf.at[i, c, down(near, k)], rbuf.at[i, k, c], pn_s.at[i, k, c], pn_r.at[i, k, c],
-            tp=near,
+            pbuf.at[i, c, down(near, k)], rbuf.at[i, c, k], pn_s.at[0], pn_r.at[i, c], tp=near
         )
 
     def p_far(i, k, c):
         q = down(t, k)
-        return remote(pbuf.at[i, c, q], fbuf.at[i, k, c], pf_s.at[i, k, c], pf_r.at[i, k, c], tp=q)
+        return remote(
+            pbuf.at[i, c, q], fbuf.at[i, k - 1, c], pf_s.at[k - 1], pf_r.at[i, k - 1, c], tp=q
+        )
 
     def back(i, c):
-        return remote(fin.at[i, c], ret.at[c, s], rz_s.at[i, c], rz_r.at[s, c], sp=i)
-
-    def back_arrival(e, c):
-        return remote(fin.at[e, c], ret.at[c, e], rz_s.at[e, c], rz_r.at[e, c], sp=e)
+        return remote(fin.at[i, c], ret.at[c, s], rz_s.at[0], rz_r.at[c], sp=i)
 
     def push(i, c):
         for k in range(1, H):
@@ -261,15 +261,15 @@
 
     def ready(p):
         i = visit(s, p, S)
-        for c in C:
-            for k in range(H):
-                near_copy(i, k, c).wait_recv()
-
-        @pl.loop(0, T)
-        def _(q):
-            @pl.when((i != s) | (q != t))
-            def _():
-                r_arrival(i, q).wait_recv()
+        whole(rbuf.at[i], n_s.at[0], n_r.at[i]).wait_recv()
+
+        @pl.when(i != s)
+        def _():
+            whole(rin.at[i], rr_s.at[0], rr_r.at[i]).wait_recv()
+
+        @pl.when(i == s)
+        def _():
+            whole(rin.at[i, pl.ds(0, T - 1)], rr_s.at[0], rr_r.at[i]).wait_recv()
 
     NT = 256 if (2 * F) % 256 == 0 else 128
     DT = 512
@@ -316,19 +316,18 @@
 
     def pair(p, c):
         i = visit(s, p, S)
-        for k in range(H):
-            p_near(i, k, c).wait_recv()
+        whole(rbuf.at[i, c], pn_s.at[0], pn_r.at[i, c]).wait_recv()
         for k in range(1, H):
             q = down(t, k)
-            pbuf[i, c, q] = (pbuf[i, c, q].astype(F32) + rbuf[i, k, c].astype(F32)).astype(BF)
+            pbuf[i, c, q] = (pbuf[i, c, q].astype(F32) + rbuf[i, c, k].astype(F32)).astype(BF)
             p_far(i, k, c).start()
 
     def finish(p, c):
         i = visit(s, p, S)
-        value = pbuf[i, c, t].astype(F32) + rbuf[i, 0, c].astype(F32)
+        value = pbuf[i, c, t].astype(F32) + rbuf[i, c, 0].astype(F32)
         for k in range(1, H):
             p_far(i, k, c).wait_recv()
-            value = value + fbuf[i, k, c].astype(F32)
+            value = value + fbuf[i, k - 1, c].astype(F32)
         return i, value.astype(BF)
 
     def send_back(p, c):
@@ -343,8 +342,7 @@
                 act(p, n)
 
     def mix_part(c, wide, square):
-        for k in range(H):
-            o_near(k, c).wait_recv()
+        whole(opj.at[c, pl.ds(0, H)], on_s.at[0], on_r.at[c]).wait_recv()
         total = jnp.dot(wide, opj[c].reshape(T * GD, DC), preferred_element_type=F32)
         mixed = (resid[:, cut(c)].astype(F32) + total).astype(BF)
         mixed_v[:, cut(c)] = mixed
@@ -368,8 +366,7 @@
     for c in range(2, NC):
         o_pass(c - 2)
         o_spread(c)
-    for j in range(1, T):
-        piece_copy(j).wait_recv()
+    whole(gout.at[pl.ds(0, T - 1)], pc_s.at[0], pc_r.at[0]).wait_recv()
     wide = jnp.concatenate([gout[q] for q in range(T)], axis=1)
     for c in C:
         square = mix_part(c, wide, square)
@@ -386,10 +383,13 @@
 
     rin[s, t] = rsend[s]
 
-    @pl.loop(1, S * T)
+    @pl.loop(1, T)
     def _(j):
-        peer = lax.rem(s * T + t + j, S * T)
-        r_copy(peer // T, lax.rem(peer, T)).start()
+        r_copy(s, lax.rem(t + j, T), 0).start()
+
+    @pl.loop(0, (S - 1) * T)
+    def _(j):
+        r_copy(lax.rem(s + 1 + j // T, S), lax.rem(j, T), 1).start()
 
     @pl.loop(jnp.where(inner, 3, 2), S)
     def _(j):
@@ -413,8 +413,8 @@
         fwd(1, 3)
         relay(1, 0)
         hidden(0, 3, 5)
+        hidden(0, 5, 7)
         relay(1, 1)
-        hidden(0, 5, 7)
         fwd(2, 0)
         gated(0)
         lower(0, 0)
@@ -428,52 +428,58 @@
         ready(1)
         hidden(1, 0, 3)
         fwd(2, 3)
+        only(inner, pair, 0, 0)
         relay(2, 0)
         hidden(1, 3, 5)
         relay(2, 1)
         hidden(1, 5, 7)
         only(edge, fwd, 3, 0)
+        gated(1)
         relay(2, 2)
-        gated(1)
         lower(1, 0)
         only(edge, fwd, 3, 1)
         lower(1, 1)
         lower(1, 2)
         only(inner, pair, 1, 0)
         relay(2, 3)
+        only(edge, fwd, 3, 2)
         lower(1, 3)
         only(inner, pair, 1, 1)
-        only(edge, fwd, 3, 2)
-        only(inner, pair, 1, 2, 3)
         only(edge, fwd, 3, 3)
+        only(edge, pair, 1, 0)
         ready(2)
+        only(inner, pair, 1, 2)
         hidden(2, 0, 3)
-        only(inner, send_back, 1, 0)
+        only(inner, pair, 1, 3)
+        only(inner, fwd, 3, 0)
         only(edge, relay, 3, 0)
-        only(inner, fwd, 3, 0)
         hidden(2, 3, 5)
         only(edge, relay, 3, 1)
         only(inner, fwd, 3, 1)
-        only(inner, send_back, 1, 1)
+        only(inner, send_back, 1, 0)
         hidden(2, 5, 7)
+        only(inner, fwd, 3, 2)
         gated(2)
         only(edge, relay, 3, 2)
-        only(inner, fwd, 3, 2)
-        only(inner, send_back, 1, 2)
+        only(inner, send_back, 1, 1)
         lower(2, 0)
+        only(inner, fwd, 3, 3)
         lower(2, 1)
         only(edge, pair, 2, 0)
+        only(inner, send_back, 1, 2)
         lower(2, 2)
         only(edge, pair, 2, 1)
         only(edge, relay, 3, 3)
-        only(inner, fwd, 3, 3)
         lower(2, 3)
         only(inner, send_back, 1, 3)
         only(edge, pair, 2, 2, 3)
+        only(edge, pair, 1, 1)
         only(inner, pair, 2, 0, 1, 2, 3)
+        only(inner, pair, 0, 1)
         only(inner, relay, 3, 0, 1, 2, 3)
         ready(3)
         hidden(3, 0, 3)
+        only(edge, send_back, 1, 0)
         only(edge, send_back, 2, 0)
         hidden(3, 3, 5)
         only(edge, send_back, 2, 1)
@@ -484,25 +490,25 @@
         only(inner, send_back, 2, 1)
         lower(3, 0)
         lower(3, 1)
+        lower(3, 2)
         pair(3, 0)
-        lower(3, 2)
         pair(3, 1)
         only(inner, send_back, 2, 2)
         lower(3, 3)
         only(edge, send_back, 2, 3)
         pair(3, 2)
         pair(3, 3)
-        only(edge, pair, 1, 0, 1, 2, 3)
-        pair(0, 0)
-        pair(0, 1)
+        only(edge, pair, 1, 2, 3)
+        only(edge, pair, 0, 0, 1)
         pair(0, 2)
         pair(0, 3)
         only(inner, send_back, 2, 3)
+        only(edge, send_back, 1, 1)
         send_back(3, 0)
         send_back(3, 1)
         send_back(3, 2)
         send_back(3, 3)
-        only(edge, send_back, 1, 0, 1, 2, 3)
+        only(edge, send_back, 1, 2, 3)
     else:
         @pl.loop(0, S + 1)
         def _(j):
@@ -543,10 +549,7 @@
     for c in C:
         _, value = finish(0, c)
         ret[c, s] = value
-
-        @pl.loop(1, S)
-        def _(j):
-            back_arrival(visit(s, j, S), c).wait_recv()
+        whole(ret.at[c, pl.ds(0, S - 1)], rz_s.at[0], rz_r.at[c]).wait_recv()
 
         flat = ret[c].reshape(slots, DC)
         total = mixed_v[:, cut(c)].astype(F32)
@@ -556,37 +559,22 @@
         out[:, cut(c)] = (total + (picked[0] + picked[1])).astype(BF)
 
     rim_copy.wait_send()
-    for c in C:
-        for k in range(1, H):
-            o_far(k, c).wait_send()
-            for j in range(1, G):
-                o_part(k, j, c).wait_send()
-        for k in range(H):
-            o_near(k, c).wait_send()
-    for j in range(1, T):
-        piece_copy(j).wait_send()
-
-    @pl.loop(0, S)
-    def _(i):
-        for c in C:
-            for k in range(1, H):
-                far_copy(i, k, c).wait_send()
-                p_far(i, k, c).wait_send()
-            for k in range(H):
-                near_copy(i, k, c).wait_send()
-                p_near(i, k, c).wait_send()
-
-    @pl.loop(1, S)
-    def _(j):
-        i = visit(s, j, S)
-        for c in C:
-            z_copy(i, c).wait_send()
-            back(i, c).wait_send()
-
-    @pl.loop(1, S * T)
-    def _(j):
-        peer = lax.rem(s * T + t + j, S * T)
-        r_copy(peer // T, lax.rem(peer, T)).wait_send()
+    half = opj.at[:, 0, pl.ds(0, GH)]
+    for k in range(1, H):
+        whole(half, ox_s.at[k - 1], ox_r.at[0, 0]).wait_send()
+        for j in range(1, G):
+            whole(half, oy_s.at[k - 1, j - 1], oy_r.at[0, 0, 0]).wait_send()
+        whole(fin, f_s.at[k - 1], f_r.at[0, 0, 0]).wait_send()
+        whole(fin, pf_s.at[k - 1], pf_r.at[0, 0, 0]).wait_send()
+    whole(opj.at[:, pl.ds(0, H)], on_s.at[0], on_r.at[0]).wait_send()
+    whole(piece.at[pl.ds(0, T - 1)], pc_s.at[0], pc_r.at[0]).wait_send()
+    whole(rbuf, n_s.at[0], n_r.at[0]).wait_send()
+    whole(rbuf, pn_s.at[0], pn_r.at[0, 0]).wait_send()
+    others = fin.at[pl.ds(0, S - 1)]
+    whole(others, z_s.at[0], z_r.at[0, 0]).wait_send()
+    whole(others, rz_s.at[0], rz_r.at[0]).wait_send()
+    whole(rin.at[0, pl.ds(0, T - 1)], rr_s.at[0], rr_r.at[0]).wait_send()
+    whole(rin.at[pl.ds(0, S - 1)], rr_s.at[1], rr_r.at[0]).wait_send()
 
 
 def local(
@@ -616,14 +604,14 @@
             buf(D, 2 * F), buf(F, D), buf(NC, T, GD, DC), buf(RIM, GD), buf(T, R, GD),
             buf(T, R, GD),
             buf(NC, S, SL, DC), buf(S, NC, T, SL, DC), buf(S, NC, T, SL, DC),
-            buf(S, H, NC, SL, DC), buf(S, H, NC, SL, DC), buf(S, NC, SL, DC), buf(NC, S, SL, DC),
-            pltpu.VMEM((T * SL, 2 * F), F32), buf(T * SL, F), buf(R, D), buf(R, D),
+            buf(S, NC, H, SL, DC), buf(S, H - 1, NC, SL, DC), buf(S, NC, SL, DC),
+            buf(NC, S, SL, DC),
+            pltpu.VMEM((T * SL, 2 * F), F32), buf(T * SL, F), buf(R, D),
             pltpu.VMEM((S, 1, 128), F32), pltpu.VMEM((S, T, 1, 128), F32),
-            dma(3), dma(H, NC), dma(H, NC), dma(H, G, NC), dma(H, G, NC), dma(H, NC), dma(H, NC),
-            dma(1), dma(1), dma(T), dma(T),
-            dma(S, NC), dma(S, NC), dma(S, H, NC), dma(S, H, NC), dma(S, H, NC), dma(S, H, NC),
-            dma(S, H, NC), dma(S, H, NC), dma(S, H, NC), dma(S, H, NC), dma(S, NC), dma(S, NC),
-            dma(S, T), dma(S, T),
+            dma(3), dma(H - 1), dma(H - 1, NC), dma(H - 1, G - 1), dma(H - 1, G - 1, NC),
+            dma(1), dma(NC), dma(1), dma(1), dma(1), dma(1),
+            dma(1), dma(S, NC), dma(H - 1), dma(S, H - 1, NC), dma(1), dma(S),
+            dma(1), dma(S, NC), dma(H - 1), dma(S, H - 1, NC), dma(1), dma(NC), dma(2), dma(S),
         ],
         compiler_params=pltpu.CompilerParams(
             collective_id=0, has_side_effects=True, vmem_limit_bytes=63 * 1024 * 1024

time: 88.1 us -> 81.6 us (0.926)
  Pallas kernels: 86 us -> 79.6 us
    pallas_call x1, Pallas kernels: 86 us -> 79.6 us  [local(): pl.pallas_call(functools.partial(kernel, G, S, T, R, SL, NC), out_shape=j...]
where the time goes in v2:
time: 81.6 us; the launch traced here: 81.5 us
  Pallas kernels  79.6 us (98%)
  local copies, waits for them, and re-layouts  1.88 us (2%)
    pallas_call x1, Pallas kernels, local(): pl.pallas_call(functools.partial(kernel, G, S, T, R, SL, NC), out_shape=j...  79.6 us
    unnamed x1, local copies, waits for them, and re-layouts  1.88 us

profile of v2, /device:TPU:0, one launch (start us, length us, event | category | flops | bytes accessed | tf_op | source)
XLA Modules:
  0.0 81.5 jit_solution(15523864593582852042)
XLA Ops:
  0.0 79.6 %shard_map.109 = bf16[128,2048]{1,0:T(8,128)(2,1)} custom-call(bf16[128,2048]{1,0:T(8,128)(2,1)} %resid.1, bf16[512,128]{1,0:T(8,128)(2,1)} %pool.1, bf16[1,128,128]{2,1,0:T(8,128)(2,1)} %gmap.1, bf16[1,128]{1,0:T(2,128)(2,1)} %bitcast.11, bf16[128,2048]{1,0:T(8,128)(2,1)} %oproj.1, bf16[2048]{0:T(1024)(128)(2,1)} %gain.1, s32[2,128]{1,0:T(2,128)} %bitcast.9, ...), custom_call_target="tpu_custom_call" | custom-call | tf_op jit(solution)/shard_map/pallas_call | solution.py:598
  79.6 1.9 %copy.13 = bf16[128,2048]{1,0:T(8,128)(2,1)} copy(bf16[128,2048]{1,0:T(8,128)(2,1)} %shard_map.109) | data formatting | bytes 1048576

commit v3 on v2

--- a/solution.py
+++ b/solution.py
@@ -43,11 +43,12 @@
 
 def kernel(
     G, S, T, R, SL, NC,
-    resid, pool, gmap, scale, oproj, gain, routes_t, weight_t, wg, wu, wd,
-    out,
+    resid_h, pool_h, gmap_h, scale_h, oproj_h, gain_h, routes_h, weight_h, wg, wu, wd,
+    out_h,
+    oproj, pool, resid, gmap, scale, gain, routes_t, weight_t, out,
     wgu_v, wd_v, opj, rim, piece, gout, stage, inbox, pbuf, rbuf, fbuf, fin, ret,
     acc, hid, mixed_v, rsend, rin,
-    w_sem, ox_s, ox_r, oy_s, oy_r, on_s, on_r, rim_s, rim_r, pc_s, pc_r,
+    w_sem, i_sem, ox_s, ox_r, oy_s, oy_r, on_s, on_r, rim_s, rim_r, pc_s, pc_r,
     z_s, z_r, f_s, f_r, n_s, n_r, pn_s, pn_r, pf_s, pf_r, rz_s, rz_r, rr_s, rr_r,
 ):
     g = lax.axis_index("grp")
@@ -83,6 +84,28 @@
             device_id_type=MESH,
         )
 
+    barrier = pltpu.get_barrier_semaphore()
+
+    @pl.loop(1, S * T)
+    def _(j):
+        peer = lax.rem(s * T + t + j, S * T)
+        pl.semaphore_signal(
+            barrier, inc=1, device_id={"grp": g, "sp": peer // T, "tp": lax.rem(peer, T)},
+            device_id_type=MESH,
+        )
+
+    for j in range(1, G):
+        pl.semaphore_signal(
+            barrier, inc=1, device_id={"grp": lax.rem(g + j, G), "sp": s, "tp": t},
+            device_id_type=MESH,
+        )
+    pairs = (
+        (oproj_h, oproj), (pool_h, pool), (resid_h, resid), (gmap_h, gmap), (scale_h, scale),
+        (gain_h, gain), (routes_h, routes_t), (weight_h, weight_t),
+    )
+    takes = [pltpu.make_async_copy(a, b, i_sem.at[n]) for n, (a, b) in enumerate(pairs)]
+    for take in takes:
+        take.start()
     loads = [
         pltpu.make_async_copy(wg, wgu_v.at[:, pl.ds(0, F)], w_sem.at[0]),
         pltpu.make_async_copy(wu, wgu_v.at[:, pl.ds(F, F)], w_sem.at[1]),
@@ -91,21 +114,8 @@
     for load in loads:
         load.start()
 
-    barrier = pltpu.get_barrier_semaphore()
-
-    @pl.loop(1, S * T)
-    def _(j):
-        peer = lax.rem(s * T + t + j, S * T)
-        pl.semaphore_signal(
-            barrier, inc=1, device_id={"grp": g, "sp": peer // T, "tp": lax.rem(peer, T)},
-            device_id_type=MESH,
-        )
-
-    for j in range(1, G):
-        pl.semaphore_signal(
-            barrier, inc=1, device_id={"grp": lax.rem(g + j, G), "sp": s, "tp": t},
-            device_id_type=MESH,
-        )
+    for take in takes:
+        take.wait()
     pl.semaphore_wait(barrier, S * T - 1 + G - 1)
 
     seq = pool.shape[0]
@@ -557,6 +567,7 @@
             weight_col[k] * jnp.dot(pick[k], flat, preferred_element_type=F32) for k in range(2)
         ]
         out[:, cut(c)] = (total + (picked[0] + picked[1])).astype(BF)
+        pltpu.make_async_copy(out.at[:, cut(c)], out_h.at[:, cut(c)], w_sem.at[3]).start()
 
     rim_copy.wait_send()
     half = opj.at[:, 0, pl.ds(0, GH)]
@@ -575,6 +586,7 @@
     whole(others, rz_s.at[0], rz_r.at[0]).wait_send()
     whole(rin.at[0, pl.ds(0, T - 1)], rr_s.at[0], rr_r.at[0]).wait_send()
     whole(rin.at[pl.ds(0, S - 1)], rr_s.at[1], rr_r.at[0]).wait_send()
+    pltpu.make_async_copy(out, out_h, w_sem.at[3]).wait()
 
 
 def local(
@@ -592,15 +604,17 @@
     GD = group_map.shape[1]
     NC = 4
     DC = D // NC
-    vmem, hbm = pl.BlockSpec(memory_space=pltpu.VMEM), pl.BlockSpec(memory_space=pl.ANY)
+    hbm = pl.BlockSpec(memory_space=pl.ANY)
     dma = lambda *n: pltpu.SemaphoreType.DMA(n)
     buf = lambda *n: pltpu.VMEM(n, BF)
     return pl.pallas_call(
         functools.partial(kernel, G, S, T, R, SL, NC),
         out_shape=jax.ShapeDtypeStruct((R, D), BF),
-        in_specs=[vmem] * 8 + [hbm] * 3,
-        out_specs=vmem,
+        in_specs=[hbm] * 11,
+        out_specs=hbm,
         scratch_shapes=[
+            buf(GD, D), buf(pool_input.shape[0], GD), buf(R, D), buf(1, GD, GD), buf(1, GD), buf(D),
+            pltpu.VMEM((top, R), jnp.int32), pltpu.VMEM((top, R), F32), buf(R, D),
             buf(D, 2 * F), buf(F, D), buf(NC, T, GD, DC), buf(RIM, GD), buf(T, R, GD),
             buf(T, R, GD),
             buf(NC, S, SL, DC), buf(S, NC, T, SL, DC), buf(S, NC, T, SL, DC),
@@ -608,7 +622,7 @@
             buf(NC, S, SL, DC),
             pltpu.VMEM((T * SL, 2 * F), F32), buf(T * SL, F), buf(R, D),
             pltpu.VMEM((S, 1, 128), F32), pltpu.VMEM((S, T, 1, 128), F32),
-            dma(3), dma(H - 1), dma(H - 1, NC), dma(H - 1, G - 1), dma(H - 1, G - 1, NC),
+            dma(4), dma(8), dma(H - 1), dma(H - 1, NC), dma(H - 1, G - 1), dma(H - 1, G - 1, NC),
             dma(1), dma(NC), dma(1), dma(1), dma(1), dma(1),
             dma(1), dma(S, NC), dma(H - 1), dma(S, H - 1, NC), dma(1), dma(S),
             dma(1), dma(S, NC), dma(H - 1), dma(S, H - 1, NC), dma(1), dma(NC), dma(2), dma(S),

time: 81.6 us -> 80.9 us (level)
  no operation moved by 1% of the time
where the time goes in v3:
time: 80.9 us; the launch traced here: 80.7 us
  Pallas kernels  78.8 us (97%)
  local copies, waits for them, and re-layouts  1.88 us (2%)
    pallas_call x1, Pallas kernels, local(): pl.pallas_call(functools.partial(kernel, G, S, T, R, SL, NC), out_shape=j...  78.8 us
    unnamed x1, local copies, waits for them, and re-layouts  1.88 us

profile of v3, /device:TPU:0, one launch (start us, length us, event | category | flops | bytes accessed | tf_op | source)
XLA Modules:
  0.0 80.7 jit_solution(840875266847357607)
XLA Ops:
  0.0 78.8 %shard_map.109 = bf16[128,2048]{1,0:T(8,128)(2,1)} custom-call(bf16[128,2048]{1,0:T(8,128)(2,1)} %resid_h.1, bf16[512,128]{1,0:T(8,128)(2,1)} %pool_h.1, bf16[1,128,128]{2,1,0:T(8,128)(2,1)} %gmap_h.1, bf16[1,128]{1,0:T(2,128)(2,1)} %bitcast.11, bf16[128,2048]{1,0:T(8,128)(2,1)} %oproj_h.1, bf16[2048]{0:T(1024)(128)(2,1)} %gain_h.1, s32[2,128]{1,0:T(2,128)} %bitcast.9, ...), custom_call_target="tpu_custom_call" | custom-call | tf_op jit(solution)/shard_map/pallas_call | solution.py:610
  78.8 1.9 %copy.13 = bf16[128,2048]{1,0:T(8,128)(2,1)} copy(bf16[128,2048]{1,0:T(8,128)(2,1)} %shard_map.109) | data formatting | bytes 1048576

commit v4 on v3

--- a/solution.py
+++ b/solution.py
@@ -86,11 +86,16 @@
 
     barrier = pltpu.get_barrier_semaphore()
 
-    @pl.loop(1, S * T)
+    @pl.loop(1, S)
     def _(j):
-        peer = lax.rem(s * T + t + j, S * T)
         pl.semaphore_signal(
-            barrier, inc=1, device_id={"grp": g, "sp": peer // T, "tp": lax.rem(peer, T)},
+            barrier, inc=1, device_id={"grp": g, "sp": lax.rem(s + j, S), "tp": t},
+            device_id_type=MESH,
+        )
+
+    for j in range(1, T):
+        pl.semaphore_signal(
+            barrier, inc=1, device_id={"grp": g, "sp": s, "tp": lax.rem(t + j, T)},
             device_id_type=MESH,
         )
 
@@ -116,7 +121,7 @@
 
     for take in takes:
         take.wait()
-    pl.semaphore_wait(barrier, S * T - 1 + G - 1)
+    pl.semaphore_wait(barrier, S - 1 + T - 1 + G - 1)
 
     seq = pool.shape[0]
     rim_copy = remote(

time: 80.9 us -> 81 us (level)
  no operation moved by 1% of the time
where the time goes in v4:
time: 81 us; the launch traced here: 80.9 us
  Pallas kernels  79 us (98%)
  local copies, waits for them, and re-layouts  1.88 us (2%)
    pallas_call x1, Pallas kernels, local(): pl.pallas_call(functools.partial(kernel, G, S, T, R, SL, NC), out_shape=j...  79 us
    unnamed x1, local copies, waits for them, and re-layouts  1.88 us

profile of v4, /device:TPU:0, one launch (start us, length us, event | category | flops | bytes accessed | tf_op | source)
XLA Modules:
  0.0 80.9 jit_solution(4953865051591482761)
XLA Ops:
  0.0 79.0 %shard_map.109 = bf16[128,2048]{1,0:T(8,128)(2,1)} custom-call(bf16[128,2048]{1,0:T(8,128)(2,1)} %resid_h.1, bf16[512,128]{1,0:T(8,128)(2,1)} %pool_h.1, bf16[1,128,128]{2,1,0:T(8,128)(2,1)} %gmap_h.1, bf16[1,128]{1,0:T(2,128)(2,1)} %bitcast.11, bf16[128,2048]{1,0:T(8,128)(2,1)} %oproj_h.1, bf16[2048]{0:T(1024)(128)(2,1)} %gain_h.1, s32[2,128]{1,0:T(2,128)} %bitcast.9, ...), custom_call_target="tpu_custom_call" | custom-call | tf_op jit(solution)/shard_map/pallas_call | solution.py:615
  79.0 1.9 %copy.13 = bf16[128,2048]{1,0:T(8,128)(2,1)} copy(bf16[128,2048]{1,0:T(8,128)(2,1)} %shard_map.109) | data formatting | bytes 1048576
